TPU v7x, 32 devices: a whole 2x2x4 slice. The times are simulated.
32 devices in a mesh: sp: 8 (over z, x), tp: 4 (over y, core).
Axes of the slice: x: 2, y: 2, z: 4, core: 2. Of those that a mesh axis runs over, the one named last changes fastest.
Arguments:
- tokens: bfloat16 [1024, 2048], P('sp'), may hold values from -6 to 6
- query_narrow: bfloat16 [1024, 2048], P('sp', 'tp'), may hold values from -20 to 20
- key_narrow: bfloat16 [1024, 2048], P('sp', 'tp'), may hold values from -20 to 20
- value_narrow: bfloat16 [1024, 2048], P('sp', 'tp'), may hold values from -6 to 6
- query_broad: bfloat16 [1024, 4096], P('sp', 'tp'), may hold values from -20 to 20
- key_broad: bfloat16 [1024, 4096], P('sp', 'tp'), may hold values from -20 to 20
- value_broad: bfloat16 [1024, 2048], P('sp', 'tp'), may hold values from -6 to 6
- mix_lambda: float32 [2, 16], P(None, 'tp'), may hold values from 0.3 to 0.8
- head_gain: float32 [2, 128], replicated, may hold values from 0.1 to 1.9
- proj_narrow: bfloat16 [2048, 2048], P('tp'), may hold values from -0.09375 to 0.09375
- proj_broad: bfloat16 [2048, 2048], P('tp'), may hold values from -0.09375 to 0.09375
- gain_one: float32 [2048], replicated, may hold values from 0.1 to 1.9
- gain_two: float32 [2048], replicated, may hold values from 0.1 to 1.9
- expert_ids: int32 [1024, 2], P('sp'), may hold values from 0 to 31, all different within a row; in each aligned block of 128 rows (0 to 127, 128 to 255, ...) at most 16 rows name the same one
- expert_gates: float32 [1024, 2], P('sp'), may hold values from 0.1 to 0.9
- gate_weight: bfloat16 [32, 2048, 4096], P('sp', None, 'tp'), may hold values from -0.125 to 0.125
- up_weight: bfloat16 [32, 2048, 4096], P('sp', None, 'tp'), may hold values from -0.125 to 0.125
- down_weight: bfloat16 [32, 4096, 2048], P('sp', 'tp'), may hold values from -0.09375 to 0.09375
Outputs:
- result: bfloat16 [1024, 2048], P('sp')
Inputs may be any that keep to these rules, and one draw needn't show every extreme that they name: `expert_ids`: the 2 experts of a token differ. Among the tokens of one index of sp (aligned blocks of 128 tokens) no expert is named by more than 16 tokens, and in some blocks one expert is named by exactly 16.
All inputs are finite; a program needn't handle non-finite values.
Results may differ from a plain program's by a relative error of at most 0.015.
Values may be sent and summed in bfloat16 or wider, within the bound.
A program may use at most 128 MiB of HBM per device.

v0:
```python
import functools

import jax
import jax.numpy as jnp
from jax import lax
from jax.experimental import pallas as pl
from jax.experimental.pallas import tpu as pltpu
from jax.sharding import PartitionSpec as P

QK_NARROW = 64
QK_BROAD = 128
V = 128
TOP = 2
CAP = 16


deep_alpha = 8.0**0.25
norm_eps = 1e-05


def layer_scale(inputs, gains):
    center = jnp.mean(inputs, -1, keepdims=True)
    spread = jnp.mean(jnp.square(inputs - center), -1, keepdims=True)
    return (inputs - center) * lax.rsqrt(spread + norm_eps) * gains


MESH = pl.DeviceIdType.MESH
LOG2E = 1.4426950408889634


def remote(src, dst, send, recv, axis, index):
    return pltpu.make_async_remote_copy(
        src_ref=src,
        dst_ref=dst,
        send_sem=send,
        recv_sem=recv,
        device_id={axis: index},
        device_id_type=MESH,
    )


def greet(n_sp, n_tp, sp, tp):
    barrier = pltpu.get_barrier_semaphore()
    for k in range(1, n_sp):
        pl.semaphore_signal(
            barrier, inc=1, device_id={"sp": lax.rem(sp + k, n_sp)}, device_id_type=MESH
        )
    for k in range(1, n_tp):
        pl.semaphore_signal(
            barrier, inc=1, device_id={"tp": lax.rem(tp + k, n_tp)}, device_id_type=MESH
        )
    pl.semaphore_wait(barrier, n_sp + n_tp - 2)


def lanes(index, width):
    return pl.ds(pl.multiple_of(index * width, width), width)


def attention_kernel(
    n_sp, n_tp, heads, lam, tok, qn, kn, vn, qb, kb, vb, gains, pn, pb, gain_one,
    out, q_all, k_all, v_all, head_out, head_in, proj_n, proj_b, part, part_in, attn,
    send, recv, own, head_send, head_recv, tp_send, tp_recv, weights,
):
    sp, tp = lax.axis_index("sp"), lax.axis_index("tp")
    count = tok.shape[0]
    width = part.shape[2]
    lane = V

    def group_of(s):
        return (s + s // 2) % 2

    load_n = pltpu.make_async_copy(pn, proj_n, weights.at[0])
    load_b = pltpu.make_async_copy(pb, proj_b, weights.at[1])
    load_n.start()
    load_b.start()
    greet(n_sp, n_tp, sp, tp)
    rows = pl.ds(pl.multiple_of(sp * count, count), count)

    def pieces(grp, head):
        cut = lanes(head, lane)
        if grp == 0:
            return (
                (qn.at[:, cut], q_all.at[rows, 0:lane]),
                (kn.at[:, cut], k_all.at[rows, 0:lane]),
                (vn.at[:, cut], v_all.at[rows]),
            )
        return (
            (qb.at[:, lanes(head, 2 * lane)], q_all.at[rows]),
            (kb.at[:, lanes(head, 2 * lane)], k_all.at[rows]),
            (vb.at[:, cut], v_all.at[rows]),
        )

    for k in range(1, n_sp):
        to = lax.rem(sp + k, n_sp)
        for grp in range(2):

            @pl.when(group_of(to) == grp)
            def _():
                for i, (a, b) in enumerate(pieces(grp, to // 2)):
                    remote(a, b, send.at[i, k], recv.at[i, k], "sp", to).start()

    my_group, my_head = group_of(sp), sp // 2
    for grp in range(2):

        @pl.when(my_group == grp)
        def _():
            for i, (a, b) in enumerate(pieces(grp, my_head)):
                pltpu.make_async_copy(a, b, own.at[i]).start()
            for i, (a, b) in enumerate(pieces(grp, my_head)):
                pltpu.make_async_copy(a, b, own.at[i]).wait()
            for k in range(1, n_sp):
                source = lax.rem(sp + n_sp - k, n_sp)
                from_rows = pl.ds(pl.multiple_of(source * count, count), count)
                size = lane * (grp + 1)
                for i, b in enumerate(
                    (
                        q_all.at[from_rows, 0:size],
                        k_all.at[from_rows, 0:size],
                        v_all.at[from_rows],
                    )
                ):
                    remote(b, b, send.at[i, k], recv.at[i, k], "sp", source).wait_recv()

    factor = jnp.where(my_group == 0, QK_NARROW**-0.5, QK_BROAD**-0.5) * LOG2E
    mixing = lam[my_group, my_head]
    gain = gains[pl.ds(my_group, 1), :]
    span = 2 * count
    col = my_group * heads + my_head
    keep_all = jnp.broadcast_to(my_group, (span, lane)) == 1
    place = lax.broadcasted_iota(jnp.int32, (span, lane), 1) // QK_NARROW
    for block in range(n_sp // 2):
        q_rows = slice(block * span, (block + 1) * span)
        parts = []
        for m in range(2):
            cut = lanes(my_group * m, lane)
            queries = q_all[q_rows, cut].astype(jnp.float32)
            queries = jnp.where(keep_all | (place == m), queries, 0.0).astype(jnp.bfloat16)
            scores = lax.dot_general(
                queries, k_all[:, cut], (((1,), (1,)), ((), ())),
                preferred_element_type=jnp.float32,
            )
            highest = jnp.max(scores, -1, keepdims=True)
            expo = jnp.exp2((scores - highest) * factor)
            total = jnp.sum(expo, -1, keepdims=True)
            numer = jnp.dot(
                expo.astype(jnp.bfloat16), v_all[...], preferred_element_type=jnp.float32
            )
            parts.append(numer / total)
        diff = parts[0] - mixing * parts[1]
        normed = diff * lax.rsqrt(jnp.mean(diff * diff, -1, keepdims=True) + norm_eps) * gain
        head_out[q_rows, :] = normed.astype(jnp.bfloat16)
        for s in (2 * block, 2 * block + 1):
            piece = head_out.at[s * count : (s + 1) * count, :]
            target = head_in.at[:, lanes(col, lane)]

            @pl.when(sp != s)
            def _():
                remote(piece, target, head_send.at[s], head_recv.at[sp], "sp", s).start()

            @pl.when(sp == s)
            def _():
                copy = pltpu.make_async_copy(piece, target, own.at[0])
                copy.start()
                copy.wait()

    load_n.wait()
    load_b.wait()
    for s in range(n_sp):
        place_s = (group_of(s) * heads + s // 2) * lane
        target = head_in.at[:, place_s : place_s + lane]

        @pl.when(sp != s)
        def _():
            remote(target, target, head_send.at[s], head_recv.at[s], "sp", s).wait_recv()

    half = heads * lane
    for k in range(n_tp):
        to = lax.rem(tp + 1 + k, n_tp)
        cut = lanes(to, width)
        product = jnp.dot(
            head_in[:, :half], proj_n[:, cut], preferred_element_type=jnp.float32
        ) + jnp.dot(head_in[:, half:], proj_b[:, cut], preferred_element_type=jnp.float32)
        if k < n_tp - 1:
            part[k] = product.astype(jnp.bfloat16)
            remote(part.at[k], part_in.at[k], tp_send.at[0, k], tp_recv.at[0, k], "tp", to).start()
    summed = product
    for k in range(n_tp - 1):
        peer = lax.rem(tp + 2 * n_tp - 1 - k, n_tp)
        remote(
            part.at[k], part_in.at[k], tp_send.at[0, k], tp_recv.at[0, k], "tp", peer
        ).wait_recv()
        summed = summed + part_in[k].astype(jnp.float32)
    mine = lanes(tp, width)
    attn[:, mine] = summed.astype(jnp.bfloat16)
    for k in range(n_tp - 1):
        to = lax.rem(tp + 1 + k, n_tp)
        remote(
            attn.at[:, mine], attn.at[:, mine], tp_send.at[1, k], tp_recv.at[1, k], "tp", to
        ).start()
    for k in range(n_tp - 1):
        peer = lax.rem(tp + 2 * n_tp - 1 - k, n_tp)
        piece = attn.at[:, lanes(peer, width)]
        remote(piece, piece, tp_send.at[1, k], tp_recv.at[1, k], "tp", peer).wait_recv()
    full = deep_alpha * tok[...].astype(jnp.float32) + attn[...].astype(jnp.float32)
    out[...] = layer_scale(full, gain_one[...]).astype(jnp.bfloat16)

    for k in range(1, n_sp):
        to = lax.rem(sp + k, n_sp)
        for grp in range(2):

            @pl.when(group_of(to) == grp)
            def _():
                for i, (a, b) in enumerate(pieces(grp, to // 2)):
                    remote(a, b, send.at[i, k], recv.at[i, k], "sp", to).wait_send()

    for s in range(n_sp):
        piece = head_out.at[s * count : (s + 1) * count, :]

        @pl.when(sp != s)
        def _():
            remote(piece, piece, head_send.at[s], head_recv.at[s], "sp", s).wait_send()

    for k in range(n_tp - 1):
        to = lax.rem(tp + 1 + k, n_tp)
        remote(
            part.at[k], part_in.at[k], tp_send.at[0, k], tp_recv.at[0, k], "tp", to
        ).wait_send()
        remote(
            attn.at[:, mine], attn.at[:, mine], tp_send.at[1, k], tp_recv.at[1, k], "tp", to
        ).wait_send()


def attention_rows(
    tokens, qn, kn, vn, qb, kb, vb, mix_lambda, head_gain, proj_n, proj_b, gain_one
):
    n_sp, n_tp = lax.axis_size("sp"), lax.axis_size("tp")
    count, model_width = tokens.shape
    heads = vn.shape[1] // V
    width = model_width // n_tp
    dma = pltpu.SemaphoreType.DMA
    bf16 = jnp.bfloat16
    far = pl.BlockSpec(memory_space=pl.ANY)
    near = pl.BlockSpec(memory_space=pltpu.VMEM)
    return pl.pallas_call(
        functools.partial(attention_kernel, n_sp, n_tp, heads),
        out_shape=jax.ShapeDtypeStruct(tokens.shape, bf16),
        in_specs=[pl.BlockSpec(memory_space=pltpu.SMEM), near]
        + [far] * 6
        + [near, far, far, near],
        out_specs=near,
        scratch_shapes=[
            pltpu.VMEM((n_sp * count, 2 * V), bf16),
            pltpu.VMEM((n_sp * count, 2 * V), bf16),
            pltpu.VMEM((n_sp * count, V), bf16),
            pltpu.VMEM((n_sp * count, V), bf16),
            pltpu.VMEM((count, 2 * heads * V), bf16),
            pltpu.VMEM(proj_n.shape, bf16),
            pltpu.VMEM(proj_b.shape, bf16),
            pltpu.VMEM((n_tp, count, width), bf16),
            pltpu.VMEM((n_tp, count, width), bf16),
            pltpu.VMEM((count, model_width), bf16),
            dma((3, n_sp)),
            dma((3, n_sp)),
            dma((3,)),
            dma((n_sp,)),
            dma((n_sp,)),
            dma((2, n_tp)),
            dma((2, n_tp)),
            dma((2,)),
        ],
        compiler_params=pltpu.CompilerParams(
            collective_id=0, has_side_effects=True, vmem_limit_bytes=40 * 2**20
        ),
        name="attention",
    )(mix_lambda, tokens, qn, kn, vn, qb, kb, vb, head_gain, proj_n, proj_b, gain_one[None, :])


def expert_kernel(
    n_sp, n_tp, mixed, spread, high, low, gain_two, wg, wu, wd, out,
    gate, up, down, rows_out, rows_in, act, part, part_core, part_far, summed, back, routed,
    loaded, a_send, a_recv, y_send, y_recv, c_send, c_recv,
    d_send, d_recv, s_send, s_recv, b_send, b_recv, g_send, g_recv,
):
    sp, tp = lax.axis_index("sp"), lax.axis_index("tp")
    experts, slots, width = rows_out.shape[1:]
    hidden = act.shape[1]
    filled = n_sp * slots
    pairs = n_tp // 2
    y, c = tp // 2, tp % 2
    other = 2 * y + 1 - c

    def load(e, go):
        for i, (a, b) in enumerate(((wg, gate), (wu, up), (wd, down))):
            copy = pltpu.make_async_copy(a.at[e], b.at[e], loaded.at[i, e])
            copy.start() if go else copy.wait()

    def each(body):
        lax.fori_loop(0, experts, lambda e, _: (body(e), 0)[1], 0)

    each(lambda e: load(e, True))
    greet(n_sp, n_tp, sp, tp)

    mine = lanes(tp, width)
    picked = jnp.dot(spread[...], mixed[:, mine], preferred_element_type=jnp.float32)
    rows_out[...] = picked.astype(jnp.bfloat16).reshape(rows_out.shape)

    def dispatch(e, k):
        to = lax.rem(sp + k, n_sp)
        return remote(
            rows_out.at[to, e], rows_in.at[tp, e, sp], a_send.at[e, k], a_recv.at[e, k], "sp", to
        )

    def send_rows(e):
        for k in range(1, n_sp):
            dispatch(e, k).start()
        rows_in[tp, e, sp] = rows_out[sp, e]

    each(send_rows)

    def far(e, k):
        block = rows_in.at[tp, e]
        to = 2 * lax.rem(y + k, pairs) + c
        return remote(block, block, y_send.at[e, k], y_recv.at[e, k], "tp", to)

    def far_slot(k):
        return 2 * lax.rem(y + pairs - k, pairs) + c

    def across(e, k):
        block = rows_in.at[far_slot(k), e]
        return remote(block, block, c_send.at[e, k], c_recv.at[e, k], "tp", other)

    def pass_on(e):
        for k in range(1, n_sp):
            source = lax.rem(sp + n_sp - k, n_sp)
            block = rows_in.at[tp, e, source]
            remote(block, block, a_send.at[e, k], a_recv.at[e, k], "sp", source).wait_recv()
        for k in range(1, pairs):
            far(e, k).start()
        across(e, 0).start()

    each(pass_on)

    def pass_across(e):
        for k in range(1, pairs):
            block = rows_in.at[far_slot(k), e]
            remote(block, block, y_send.at[e, k], y_recv.at[e, k], "tp", far_slot(k)).wait_recv()
            across(e, k).start()

    def to_core(e, k):
        yy = lax.rem(y + k, pairs)
        return remote(
            part.at[2 * yy + 1 - c, e], part_core.at[k, e], d_send.at[e, k], d_recv.at[e, k],
            "tp", other,
        )

    def to_far(e, k):
        to = 2 * lax.rem(y + k, pairs) + c
        return remote(
            part.at[to, e], part_far.at[k, e], s_send.at[e, k], s_recv.at[e, k], "tp", to
        )

    def give_back(e, k):
        to = lax.rem(sp + k, n_sp)
        return remote(
            summed.at[e, to], back.at[sp, e], b_send.at[e, k], b_recv.at[e, k], "sp", to
        )

    tile = min(256, hidden)

    def compute(e):
        pass_across(e)
        load(e, False)
        for k in range(pairs):
            block = rows_in.at[2 * lax.rem(y + pairs - k, pairs) + 1 - c, e]
            remote(block, block, c_send.at[e, k], c_recv.at[e, k], "tp", other).wait_recv()
        inputs = jnp.concatenate(
            [rows_in[t, e].reshape(filled, width) for t in range(n_tp)], axis=1
        )

        def hidden_tile(j, _):
            cut = lanes(j, tile)
            gated = jnp.dot(inputs, gate[e, :, cut], preferred_element_type=jnp.float32)
            lifted = jnp.dot(inputs, up[e, :, cut], preferred_element_type=jnp.float32)
            act[:, cut] = (gated / (1.0 + jnp.exp(-gated)) * lifted).astype(jnp.bfloat16)
            return 0

        lax.fori_loop(0, hidden // tile, hidden_tile, 0)

        def down_tile(t, _):
            product = jnp.dot(
                act[...], down[e, :, lanes(t, width)], preferred_element_type=jnp.float32
            )
            part[t, e] = product.astype(jnp.bfloat16)
            return 0

        lax.fori_loop(0, n_tp, down_tile, 0)
        for k in range(pairs):
            to_core(e, k).start()

    def core_sum(e, k):
        block = part_core.at[k, e]
        remote(block, block, d_send.at[e, k], d_recv.at[e, k], "tp", other).wait_recv()
        slot = 2 * lax.rem(y + k, pairs) + c
        return part[slot, e].astype(jnp.float32) + part_core[k, e].astype(jnp.float32)

    def reduce_core(e):
        for k in range(1, pairs):
            total = core_sum(e, k)
            part[2 * lax.rem(y + k, pairs) + c, e] = total.astype(jnp.bfloat16)
            to_far(e, k).start()

    def reduce_far(e):
        total = core_sum(e, 0)
        for k in range(1, pairs):
            block = part_far.at[k, e]
            remote(block, block, s_send.at[e, k], s_recv.at[e, k], "tp", far_slot(k)).wait_recv()
            total = total + part_far[k, e].astype(jnp.float32)
        summed[e] = total.astype(jnp.bfloat16).reshape(n_sp, slots, width)
        for k in range(1, n_sp):
            give_back(e, k).start()
        back[sp, e] = summed[e, sp]

    def step(e, _):
        pl.when(e < experts)(lambda: compute(e))
        pl.when((e >= 1) & (e <= experts))(lambda: reduce_core(e - 1))
        pl.when(e >= 2)(lambda: reduce_far(e - 2))
        return 0

    lax.fori_loop(0, experts + 2, step, 0)

    def arrive(e):
        for k in range(1, n_sp):
            source = lax.rem(sp + n_sp - k, n_sp)
            block = back.at[source, e]
            remote(block, block, b_send.at[e, k], b_recv.at[e, k], "sp", source).wait_recv()

    each(arrive)
    returned = back[...].reshape(n_sp * experts * slots, width)
    weighted = jnp.dot(high[...], returned, preferred_element_type=jnp.float32) + jnp.dot(
        low[...], returned, preferred_element_type=jnp.float32
    )
    routed[:, mine] = weighted.astype(jnp.bfloat16)

    def share(k):
        to = lax.rem(tp + k, n_tp)
        block = routed.at[:, mine]
        return remote(block, block, g_send.at[k], g_recv.at[k], "tp", to)

    for k in range(1, n_tp):
        share(k).start()
    for k in range(1, n_tp):
        peer = lax.rem(tp + n_tp - k, n_tp)
        block = routed.at[:, lanes(peer, width)]
        remote(block, block, g_send.at[k], g_recv.at[k], "tp", peer).wait_recv()
    full = deep_alpha * mixed[...].astype(jnp.float32) + routed[...].astype(jnp.float32)
    out[...] = layer_scale(full, gain_two[...]).astype(jnp.bfloat16)

    def sent(e):
        for k in range(1, n_sp):
            dispatch(e, k).wait_send()
            give_back(e, k).wait_send()
        for k in range(pairs):
            across(e, k).wait_send()
            to_core(e, k).wait_send()
        for k in range(1, pairs):
            far(e, k).wait_send()
            to_far(e, k).wait_send()

    each(sent)
    for k in range(1, n_tp):
        share(k).wait_send()


def expert_rows(mixed, spread, high, low, gain_two, wg, wu, wd):
    n_sp, n_tp = lax.axis_size("sp"), lax.axis_size("tp")
    count, model_width = mixed.shape
    experts, hidden = wg.shape[0], wg.shape[2]
    width, pairs, filled = model_width // n_tp, n_tp // 2, n_sp * CAP
    bf16 = jnp.bfloat16
    dma = pltpu.SemaphoreType.DMA
    far = pl.BlockSpec(memory_space=pl.ANY)
    near = pl.BlockSpec(memory_space=pltpu.VMEM)
    vmem = lambda *shape: pltpu.VMEM(shape, bf16)
    return pl.pallas_call(
        functools.partial(expert_kernel, n_sp, n_tp),
        out_shape=jax.ShapeDtypeStruct(mixed.shape, bf16),
        in_specs=[near] * 5 + [far] * 3,
        out_specs=near,
        scratch_shapes=[
            vmem(*wg.shape),
            vmem(*wu.shape),
            vmem(*wd.shape),
            vmem(n_sp, experts, CAP, width),
            vmem(n_tp, experts, n_sp, CAP, width),
            vmem(filled, hidden),
            vmem(n_tp, experts, filled, width),
            vmem(pairs, experts, filled, width),
            vmem(pairs, experts, filled, width),
            vmem(experts, n_sp, CAP, width),
            vmem(n_sp, experts, CAP, width),
            vmem(count, model_width),
            dma((3, experts)),
        ]
        + [dma((experts, n_sp))] * 2
        + [dma((experts, pairs))] * 8
        + [dma((experts, n_sp))] * 2
        + [dma((n_tp,))] * 2,
        compiler_params=pltpu.CompilerParams(
            collective_id=1, has_side_effects=True, vmem_limit_bytes=67043328
        ),
        name="experts",
    )(mixed, spread, high, low, gain_two[None, :], wg, wu, wd)


def head_fold(running, queries, key_rows, values, key_width):
    maxima, totals, weighted = running
    length = key_rows.shape[0]
    head_count = queries.shape[1]
    keyed = key_rows.reshape(length, head_count, 2, key_width)
    valued = values.reshape(length, head_count, V)
    scores = jnp.einsum(
        "qhmd,khmd->hmqk", queries, keyed, preferred_element_type=jnp.float32
    ) * key_width ** (-0.5)
    updated = jnp.maximum(maxima, jnp.max(scores, -1))
    exponent = jnp.exp(scores - updated[..., None])
    totals = jnp.sum(exponent, -1)
    weighted = jnp.einsum(
        "hmqk,khv->hmqv", exponent.astype(jnp.bfloat16), valued, preferred_element_type=jnp.float32
    )
    return (updated, totals, weighted)


def head_output(running, mixing, gains):
    maxima, totals, weighted = running
    diff = (
        weighted[:, 0] / totals[:, 0, :, None]
        - mixing[:, None, None] * weighted[:, 1] / totals[:, 1, :, None]
    )
    normed = (diff * lax.rsqrt(jnp.mean(diff * diff, -1, keepdims=True) + norm_eps) * gains).astype(
        jnp.bfloat16
    )
    return jnp.moveaxis(normed, 0, 1).reshape(normed.shape[1], -1)


def attention_gathered(
    tokens,
    query_narrow,
    key_narrow,
    value_narrow,
    query_broad,
    key_broad,
    value_broad,
    mix_lambda,
    head_gain,
    proj_narrow,
    proj_broad,
    gain_one,
):
    token_count = tokens.shape[0]
    head_count = value_narrow.shape[1] // V
    queries_first = query_narrow.reshape(token_count, head_count, 2, QK_NARROW)
    queries_second = query_broad.reshape(token_count, head_count, 2, QK_BROAD)
    start_state = (
        jnp.full((head_count, 2, token_count), -1e30, jnp.float32),
        jnp.zeros((head_count, 2, token_count), jnp.float32),
        jnp.zeros((head_count, 2, token_count, V), jnp.float32),
    )
    state_first = head_fold(
        start_state,
        queries_first,
        lax.all_gather(key_narrow, "sp", axis=0, tiled=True),
        lax.all_gather(value_narrow, "sp", axis=0, tiled=True),
        QK_NARROW,
    )
    state_second = head_fold(
        start_state,
        queries_second,
        lax.all_gather(key_broad, "sp", axis=0, tiled=True),
        lax.all_gather(value_broad, "sp", axis=0, tiled=True),
        QK_BROAD,
    )
    heads_first = head_output(state_first, mix_lambda[0], head_gain[0])
    heads_second = head_output(state_second, mix_lambda[1], head_gain[1])
    partial_value = jnp.dot(heads_first, proj_narrow, preferred_element_type=jnp.float32)
    partial_value = partial_value + jnp.dot(
        heads_second, proj_broad, preferred_element_type=jnp.float32
    )
    attn = lax.psum(
        partial_value.astype(jnp.bfloat16).astype(jnp.float32).astype(jnp.bfloat16), "tp"
    ).astype(jnp.float32)
    return layer_scale(deep_alpha * tokens.astype(jnp.float32) + attn, gain_one).astype(
        jnp.bfloat16
    )


def on_device(
    tokens,
    query_narrow,
    key_narrow,
    value_narrow,
    query_broad,
    key_broad,
    value_broad,
    mix_lambda,
    head_gain,
    proj_narrow,
    proj_broad,
    gain_one,
    gain_two,
    expert_ids,
    expert_gates,
    gate_weight,
    up_weight,
    down_weight,
):
    token_count = tokens.shape[0]
    model_width = tokens.shape[1]
    members = (
        tokens,
        query_narrow,
        key_narrow,
        value_narrow,
        query_broad,
        key_broad,
        value_broad,
        mix_lambda,
        head_gain,
        proj_narrow,
        proj_broad,
        gain_one,
    )
    whole_heads = 2 * (value_narrow.shape[1] // V) == lax.axis_size("sp")
    mixed_rows = (attention_rows if whole_heads else attention_gathered)(*members)
    experts_all = gate_weight.shape[0] * lax.axis_size("sp")
    chosen = expert_ids.reshape(-1)
    onehot = (chosen[:, None] == jnp.arange(experts_all, dtype=jnp.int32)[None, :]).astype(
        jnp.int32
    )
    before = jnp.cumsum(onehot, axis=0, dtype=jnp.int32) - onehot
    slot_index = jnp.sum(before * onehot, axis=-1, dtype=jnp.int32)
    position = (chosen * CAP + slot_index).reshape(expert_ids.shape)
    match = position[:, :, None] == jnp.arange(CAP * experts_all, dtype=jnp.int32)
    spread = jnp.any(match, axis=1).astype(jnp.bfloat16).T
    shares = jnp.sum(jnp.where(match, expert_gates[:, :, None], 0.0), axis=1)
    high = lax.reduce_precision(shares, 8, 7)
    low = (shares - high).astype(jnp.bfloat16)
    return expert_rows(
        mixed_rows,
        spread,
        high.astype(jnp.bfloat16),
        low,
        gain_two,
        gate_weight,
        up_weight,
        down_weight,
    )


def solution(mesh):
    return jax.shard_map(
        on_device,
        mesh=mesh,
        in_specs=(
            P("sp", None),
            P("sp", "tp"),
            P("sp", "tp"),
            P("sp", "tp"),
            P("sp", "tp"),
            P("sp", "tp"),
            P("sp", "tp"),
            P(None, "tp"),
            P(),
            P("tp", None),
            P("tp", None),
            P(),
            P(),
            P("sp", None),
            P("sp", None),
            P("sp", None, "tp"),
            P("sp", None, "tp"),
            P("sp", "tp", None),
        ),
        out_specs=P("sp", None),
        check_vma=False,
    )
```

profile of v0, /device:TPU:1, one launch (start us, length us, event | category | flops | bytes accessed | tf_op | source)
XLA Modules:
  0.0 131.2 jit_solution(5408325793977852775)
XLA Ops:
  0.0 0.8 copy.34
  0.8 0.1 eq.42
  0.9 0.1 eq.38
  1.1 0.6 reduce-window.6
  1.7 0.2 slice_reduce_fusion
  1.9 0.1 fusion.4
  2.0 0.1 reduce_sum.21
  2.2 0.1 copy.37
  2.2 0.7 multiply_add_fusion
  2.9 0.1 fusion
  3.0 0.2 copy.38
  3.2 0.7 convert_bitcast_fusion.spread
  3.9 0.8 select_reduce_fusion
  4.7 0.7 fusion.1
  5.5 0.0 copy-start.1
  5.5 1.6 %copy-done.1 = bf16[512,2048]{1,0:T(8,128)(2,1)S(1)} copy-done((bf16[512,2048]{1,0:T(8,128)(2,1)S(1)}, bf16[512,2048]{1,0:T(8,128)(2,1)}, u32[]{:S(2)}) %copy-start.1) | copy-done | bytes 2097176
  7.1 0.0 copy-start.2
  7.1 1.6 %copy-done.2 = bf16[512,2048]{1,0:T(8,128)(2,1)S(1)} copy-done((bf16[512,2048]{1,0:T(8,128)(2,1)S(1)}, bf16[512,2048]{1,0:T(8,128)(2,1)}, u32[]{:S(2)}) %copy-start.2) | copy-done | bytes 2097176
  8.7 0.0 copy-start.3
  8.7 1.0 copy-done.3
  9.7 0.0 copy-start.4
  9.7 0.9 copy-done.4
  10.7 0.0 copy-start.5
  10.7 0.9 copy-done.5
  11.6 0.0 copy-start.6
  11.6 0.9 copy-done.6
  12.5 0.0 copy-start.7
  12.5 0.9 copy-done.7
  13.4 0.0 copy-start.8
  13.4 0.9 copy-done.8
  14.3 0.0 copy-start.9
  14.3 0.9 copy-done.9
  15.2 0.0 copy-start.10
  15.2 0.7 copy-done.10
  15.9 0.0 copy-start.11
  15.9 0.7 copy-done.11
  16.6 0.0 copy-start.12
  16.6 0.7 copy-done.12
  17.3 52.9 %attention.1.mixed = bf16[128,2048]{1,0:T(8,128)(2,1)S(1)} custom-call(f32[2,4]{1,0:T(2,128)S(1)} %copy-done.11, bf16[128,2048]{1,0:T(8,128)(2,1)S(1)} %copy-done.3, bf16[128,512]{1,0:T(8,128)(2,1)S(1)} %copy-done.6, bf16[128,512]{1,0:T(8,128)(2,1)S(1)} %copy-done.7, bf16[128,512]{1,0:T(8,128)(2,1)S(1)} %copy-done.8, bf16[128,1024]{1,0:T(8,128)(2,1)S(1)} %copy-done.4, ...), custom_call_target="tpu_custom_call" | custom-call | tf_op jit(solution)/shard_map/attention/pallas_call | solution.py:244
  70.2 0.0 copy-start
  70.2 0.8 copy-done
  71.0 58.3 %experts.1 = bf16[128,2048]{1,0:T(8,128)(2,1)} custom-call(bf16[128,2048]{1,0:T(8,128)(2,1)} %copy-done, bf16[512,128]{1,0:T(8,128)(2,1)} %convert_bitcast_fusion.spread, bf16[128,512]{1,0:T(8,128)(2,1)} %get-tuple-element.6.high, bf16[128,512]{1,0:T(8,128)(2,1)} %get-tuple-element.5.low, f32[1,2048]{1,0:T(1,128)} %bitcast.24, bf16[4,2048,1024]{2,1,0:T(8,128)(2,1)} %wg.1, ...), custom_call_target="tpu_custom_call" | custom-call | tf_op jit(solution)/shard_map/experts/pallas_call | solution.py:484
  129.4 1.9 %copy.42 = bf16[128,2048]{1,0:T(8,128)(2,1)} copy(bf16[128,2048]{1,0:T(8,128)(2,1)} %experts.1) | data formatting | bytes 1048576
  (3 shorter events, 0.0 us)
Async XLA Ops:
  5.5 1.6 %copy-start.1 = (bf16[512,2048]{1,0:T(8,128)(2,1)S(1)}, bf16[512,2048]{1,0:T(8,128)(2,1)}, u32[]{:S(2)}) copy-start(bf16[512,2048]{1,0:T(8,128)(2,1)} %pn.1) | copy-start | bytes 6291460
  7.1 1.6 %copy-start.2 = (bf16[512,2048]{1,0:T(8,128)(2,1)S(1)}, bf16[512,2048]{1,0:T(8,128)(2,1)}, u32[]{:S(2)}) copy-start(bf16[512,2048]{1,0:T(8,128)(2,1)} %pb.1) | copy-start | bytes 6291460
  8.7 1.0 copy-start.3
  9.7 0.9 copy-start.4
  10.7 0.9 copy-start.5
  11.6 0.9 copy-start.6
  12.5 0.9 copy-start.7
  13.4 0.9 copy-start.8
  14.3 0.9 copy-start.9
  15.2 0.7 copy-start.10
  15.9 0.7 copy-start.11
  16.6 0.7 copy-start.12
  70.2 0.8 copy-start
where the time goes:
time: 132 us; the launch traced here: 131 us
  Pallas kernels  111 us (84%)
  local copies, waits for them, and re-layouts  16.1 us (12%)
  other arithmetic  3.81 us (3%)
    pallas_call x1, Pallas kernels, expert_rows(): pl.pallas_call(functools.partial(expert_kernel, n_sp, n_tp), out_shape=ja...  58.3 us
    pallas_call x1, Pallas kernels, attention_rows(): pl.pallas_call(functools.partial(attention_kernel, n_sp, n_tp, heads), ou...  52.9 us
    unnamed x28, local copies, waits for them, and re-layouts  15.2 us

commit v1 on v0

--- a/solution.py
+++ b/solution.py
@@ -54,225 +54,6 @@
 
 def lanes(index, width):
     return pl.ds(pl.multiple_of(index * width, width), width)
-
-
-def attention_kernel(
-    n_sp, n_tp, heads, lam, tok, qn, kn, vn, qb, kb, vb, gains, pn, pb, gain_one,
-    out, q_all, k_all, v_all, head_out, head_in, proj_n, proj_b, part, part_in, attn,
-    send, recv, own, head_send, head_recv, tp_send, tp_recv, weights,
-):
-    sp, tp = lax.axis_index("sp"), lax.axis_index("tp")
-    count = tok.shape[0]
-    width = part.shape[2]
-    lane = V
-
-    def group_of(s):
-        return (s + s // 2) % 2
-
-    load_n = pltpu.make_async_copy(pn, proj_n, weights.at[0])
-    load_b = pltpu.make_async_copy(pb, proj_b, weights.at[1])
-    load_n.start()
-    load_b.start()
-    greet(n_sp, n_tp, sp, tp)
-    rows = pl.ds(pl.multiple_of(sp * count, count), count)
-
-    def pieces(grp, head):
-        cut = lanes(head, lane)
-        if grp == 0:
-            return (
-                (qn.at[:, cut], q_all.at[rows, 0:lane]),
-                (kn.at[:, cut], k_all.at[rows, 0:lane]),
-                (vn.at[:, cut], v_all.at[rows]),
-            )
-        return (
-            (qb.at[:, lanes(head, 2 * lane)], q_all.at[rows]),
-            (kb.at[:, lanes(head, 2 * lane)], k_all.at[rows]),
-            (vb.at[:, cut], v_all.at[rows]),
-        )
-
-    for k in range(1, n_sp):
-        to = lax.rem(sp + k, n_sp)
-        for grp in range(2):
-
-            @pl.when(group_of(to) == grp)
-            def _():
-                for i, (a, b) in enumerate(pieces(grp, to // 2)):
-                    remote(a, b, send.at[i, k], recv.at[i, k], "sp", to).start()
-
-    my_group, my_head = group_of(sp), sp // 2
-    for grp in range(2):
-
-        @pl.when(my_group == grp)
-        def _():
-            for i, (a, b) in enumerate(pieces(grp, my_head)):
-                pltpu.make_async_copy(a, b, own.at[i]).start()
-            for i, (a, b) in enumerate(pieces(grp, my_head)):
-                pltpu.make_async_copy(a, b, own.at[i]).wait()
-            for k in range(1, n_sp):
-                source = lax.rem(sp + n_sp - k, n_sp)
-                from_rows = pl.ds(pl.multiple_of(source * count, count), count)
-                size = lane * (grp + 1)
-                for i, b in enumerate(
-                    (
-                        q_all.at[from_rows, 0:size],
-                        k_all.at[from_rows, 0:size],
-                        v_all.at[from_rows],
-                    )
-                ):
-                    remote(b, b, send.at[i, k], recv.at[i, k], "sp", source).wait_recv()
-
-    factor = jnp.where(my_group == 0, QK_NARROW**-0.5, QK_BROAD**-0.5) * LOG2E
-    mixing = lam[my_group, my_head]
-    gain = gains[pl.ds(my_group, 1), :]
-    span = 2 * count
-    col = my_group * heads + my_head
-    keep_all = jnp.broadcast_to(my_group, (span, lane)) == 1
-    place = lax.broadcasted_iota(jnp.int32, (span, lane), 1) // QK_NARROW
-    for block in range(n_sp // 2):
-        q_rows = slice(block * span, (block + 1) * span)
-        parts = []
-        for m in range(2):
-            cut = lanes(my_group * m, lane)
-            queries = q_all[q_rows, cut].astype(jnp.float32)
-            queries = jnp.where(keep_all | (place == m), queries, 0.0).astype(jnp.bfloat16)
-            scores = lax.dot_general(
-                queries, k_all[:, cut], (((1,), (1,)), ((), ())),
-                preferred_element_type=jnp.float32,
-            )
-            highest = jnp.max(scores, -1, keepdims=True)
-            expo = jnp.exp2((scores - highest) * factor)
-            total = jnp.sum(expo, -1, keepdims=True)
-            numer = jnp.dot(
-                expo.astype(jnp.bfloat16), v_all[...], preferred_element_type=jnp.float32
-            )
-            parts.append(numer / total)
-        diff = parts[0] - mixing * parts[1]
-        normed = diff * lax.rsqrt(jnp.mean(diff * diff, -1, keepdims=True) + norm_eps) * gain
-        head_out[q_rows, :] = normed.astype(jnp.bfloat16)
-        for s in (2 * block, 2 * block + 1):
-            piece = head_out.at[s * count : (s + 1) * count, :]
-            target = head_in.at[:, lanes(col, lane)]
-
-            @pl.when(sp != s)
-            def _():
-                remote(piece, target, head_send.at[s], head_recv.at[sp], "sp", s).start()
-
-            @pl.when(sp == s)
-            def _():
-                copy = pltpu.make_async_copy(piece, target, own.at[0])
-                copy.start()
-                copy.wait()
-
-    load_n.wait()
-    load_b.wait()
-    for s in range(n_sp):
-        place_s = (group_of(s) * heads + s // 2) * lane
-        target = head_in.at[:, place_s : place_s + lane]
-
-        @pl.when(sp != s)
-        def _():
-            remote(target, target, head_send.at[s], head_recv.at[s], "sp", s).wait_recv()
-
-    half = heads * lane
-    for k in range(n_tp):
-        to = lax.rem(tp + 1 + k, n_tp)
-        cut = lanes(to, width)
-        product = jnp.dot(
-            head_in[:, :half], proj_n[:, cut], preferred_element_type=jnp.float32
-        ) + jnp.dot(head_in[:, half:], proj_b[:, cut], preferred_element_type=jnp.float32)
-        if k < n_tp - 1:
-            part[k] = product.astype(jnp.bfloat16)
-            remote(part.at[k], part_in.at[k], tp_send.at[0, k], tp_recv.at[0, k], "tp", to).start()
-    summed = product
-    for k in range(n_tp - 1):
-        peer = lax.rem(tp + 2 * n_tp - 1 - k, n_tp)
-        remote(
-            part.at[k], part_in.at[k], tp_send.at[0, k], tp_recv.at[0, k], "tp", peer
-        ).wait_recv()
-        summed = summed + part_in[k].astype(jnp.float32)
-    mine = lanes(tp, width)
-    attn[:, mine] = summed.astype(jnp.bfloat16)
-    for k in range(n_tp - 1):
-        to = lax.rem(tp + 1 + k, n_tp)
-        remote(
-            attn.at[:, mine], attn.at[:, mine], tp_send.at[1, k], tp_recv.at[1, k], "tp", to
-        ).start()
-    for k in range(n_tp - 1):
-        peer = lax.rem(tp + 2 * n_tp - 1 - k, n_tp)
-        piece = attn.at[:, lanes(peer, width)]
-        remote(piece, piece, tp_send.at[1, k], tp_recv.at[1, k], "tp", peer).wait_recv()
-    full = deep_alpha * tok[...].astype(jnp.float32) + attn[...].astype(jnp.float32)
-    out[...] = layer_scale(full, gain_one[...]).astype(jnp.bfloat16)
-
-    for k in range(1, n_sp):
-        to = lax.rem(sp + k, n_sp)
-        for grp in range(2):
-
-            @pl.when(group_of(to) == grp)
-            def _():
-                for i, (a, b) in enumerate(pieces(grp, to // 2)):
-                    remote(a, b, send.at[i, k], recv.at[i, k], "sp", to).wait_send()
-
-    for s in range(n_sp):
-        piece = head_out.at[s * count : (s + 1) * count, :]
-
-        @pl.when(sp != s)
-        def _():
-            remote(piece, piece, head_send.at[s], head_recv.at[s], "sp", s).wait_send()
-
-    for k in range(n_tp - 1):
-        to = lax.rem(tp + 1 + k, n_tp)
-        remote(
-            part.at[k], part_in.at[k], tp_send.at[0, k], tp_recv.at[0, k], "tp", to
-        ).wait_send()
-        remote(
-            attn.at[:, mine], attn.at[:, mine], tp_send.at[1, k], tp_recv.at[1, k], "tp", to
-        ).wait_send()
-
-
-def attention_rows(
-    tokens, qn, kn, vn, qb, kb, vb, mix_lambda, head_gain, proj_n, proj_b, gain_one
-):
-    n_sp, n_tp = lax.axis_size("sp"), lax.axis_size("tp")
-    count, model_width = tokens.shape
-    heads = vn.shape[1] // V
-    width = model_width // n_tp
-    dma = pltpu.SemaphoreType.DMA
-    bf16 = jnp.bfloat16
-    far = pl.BlockSpec(memory_space=pl.ANY)
-    near = pl.BlockSpec(memory_space=pltpu.VMEM)
-    return pl.pallas_call(
-        functools.partial(attention_kernel, n_sp, n_tp, heads),
-        out_shape=jax.ShapeDtypeStruct(tokens.shape, bf16),
-        in_specs=[pl.BlockSpec(memory_space=pltpu.SMEM), near]
-        + [far] * 6
-        + [near, far, far, near],
-        out_specs=near,
-        scratch_shapes=[
-            pltpu.VMEM((n_sp * count, 2 * V), bf16),
-            pltpu.VMEM((n_sp * count, 2 * V), bf16),
-            pltpu.VMEM((n_sp * count, V), bf16),
-            pltpu.VMEM((n_sp * count, V), bf16),
-            pltpu.VMEM((count, 2 * heads * V), bf16),
-            pltpu.VMEM(proj_n.shape, bf16),
-            pltpu.VMEM(proj_b.shape, bf16),
-            pltpu.VMEM((n_tp, count, width), bf16),
-            pltpu.VMEM((n_tp, count, width), bf16),
-            pltpu.VMEM((count, model_width), bf16),
-            dma((3, n_sp)),
-            dma((3, n_sp)),
-            dma((3,)),
-            dma((n_sp,)),
-            dma((n_sp,)),
-            dma((2, n_tp)),
-            dma((2, n_tp)),
-            dma((2,)),
-        ],
-        compiler_params=pltpu.CompilerParams(
-            collective_id=0, has_side_effects=True, vmem_limit_bytes=40 * 2**20
-        ),
-        name="attention",
-    )(mix_lambda, tokens, qn, kn, vn, qb, kb, vb, head_gain, proj_n, proj_b, gain_one[None, :])
 
 
 def expert_kernel(
@@ -512,6 +293,563 @@
     )(mixed, spread, high, low, gain_two[None, :], wg, wu, wd)
 
 
+def flip(index, mask):
+    bit = 1
+    while bit <= mask:
+        if mask & bit:
+            index = index + bit - 2 * bit * lax.rem(index // bit, 2)
+        bit *= 2
+    return index
+
+
+def route(ids, gates, spread, shares, experts_all):
+    count = ids.shape[1]
+    expert = lax.broadcasted_iota(jnp.int32, (experts_all, count), 0)
+    picks = [(expert == ids[k : k + 1, :]).astype(jnp.float32) for k in range(TOP)]
+    taken = functools.reduce(lambda a, b: a + b, picks)
+    earlier = lax.broadcasted_iota(jnp.int32, (count, count), 0) < lax.broadcasted_iota(
+        jnp.int32, (count, count), 1
+    )
+    before = jnp.dot(
+        taken.astype(jnp.bfloat16),
+        earlier.astype(jnp.float32).astype(jnp.bfloat16),
+        preferred_element_type=jnp.float32,
+    )
+    place = lax.broadcasted_iota(jnp.int32, (experts_all * CAP, count), 0).astype(jnp.float32)
+    weight = jnp.zeros((experts_all * CAP, count), jnp.float32)
+    marked = jnp.zeros((experts_all * CAP, count), jnp.float32)
+    for k in range(TOP):
+        slot = jnp.sum(before * picks[k], 0, keepdims=True)
+        position = ids[k : k + 1, :].astype(jnp.float32) * CAP + slot
+        hit = place == position
+        weight = weight + jnp.where(hit, gates[k : k + 1, :], 0.0)
+        marked = marked + jnp.where(hit, 1.0, 0.0)
+    spread[...] = marked.astype(jnp.bfloat16)
+    shares[...] = weight.T.astype(jnp.bfloat16)
+
+
+def layer_kernel(
+    n_sp, n_tp, heads, lam_h, ids_h, gates_h, tok_h, qn_h, kn_h, vn_h, qb_h, kb_h, vb_h,
+    gains_h, pn_h, pb_h, one_h, two_h, wg, wu, wd, out,
+    lam, ids, gates, tok, qn, kn, vn, qb, kb, vb, gains, proj_n, proj_b, gain_one, gain_two,
+    gate, up, down, q_all, k_all, v_all, head_out, head_in, early, pc_out, pc_in, py_out, py_in,
+    st_out, st_in, mixed, spread, shares, rows_out, rows_in, act, part, part_core, part_far,
+    summed, back, z_all,
+    local, loaded, send, recv, head_send, head_recv, pc_send, pc_recv, py_send, py_recv,
+    st_send, st_recv, a_send, a_recv, y_send, y_recv, c_send, c_recv, d_send, d_recv,
+    s_send, s_recv, b_send, b_recv, g_send, g_recv,
+):
+    sp, tp = lax.axis_index("sp"), lax.axis_index("tp")
+    y, c = tp // 2, lax.rem(tp, 2)
+    core = 2 * y + 1 - c
+    far = 2 * (1 - y) + c
+    far_core = 2 * (1 - y) + 1 - c
+    count, width = tok.shape
+    lane = V
+    bf16, f32 = jnp.bfloat16, jnp.float32
+    experts, hidden = wg.shape[0], wg.shape[2]
+    slots = gate.shape[0]
+    filled = n_sp * CAP
+    mine = lanes(tp, width)
+
+    pairs = (
+        (kn_h, kn), (vn_h, vn), (kb_h, kb), (vb_h, vb), (qn_h, qn), (qb_h, qb),
+        (ids_h, ids), (gates_h, gates), (lam_h, lam), (gains_h, gains),
+        (tok_h.at[:, mine], tok), (one_h.at[:, mine], gain_one), (two_h, gain_two),
+        (pn_h, proj_n), (pb_h, proj_b),
+    )
+    copies = [pltpu.make_async_copy(a, b, local.at[i]) for i, (a, b) in enumerate(pairs)]
+    for copy in copies:
+        copy.start()
+
+    def load(e, go):
+        for i, (a, b) in enumerate(((wg, gate), (wu, up), (wd, down))):
+            slot = lax.rem(e, slots)
+            copy = pltpu.make_async_copy(a.at[e], b.at[slot], loaded.at[i, slot])
+            copy.start() if go else copy.wait()
+
+    def each(body):
+        lax.fori_loop(0, experts, lambda e, _: (body(e), 0)[1], 0)
+
+    lax.fori_loop(0, slots, lambda e, _: (load(e, True), 0)[1], 0)
+    greet(n_sp, n_tp, sp, tp)
+
+    def group_of(s):
+        return lax.rem(s + s // 2, 2)
+
+    def block_rows(s):
+        return pl.ds(pl.multiple_of(s * count, count), count)
+
+    rows = block_rows(sp)
+
+    def piece(grp, head, i):
+        size = lane * (1 if i == 2 else grp + 1)
+        source = ((qn, kn, vn), (qb, kb, vb))[grp][i]
+        return source.at[:, lanes(head, size)]
+
+    def landing(grp, s, i):
+        if i == 2:
+            return v_all.at[block_rows(s)]
+        return (q_all, k_all)[i].at[block_rows(s), 0 : lane * (grp + 1)]
+
+    def qkv(grp, k, i):
+        to = flip(sp, k)
+        return remote(
+            piece(grp, to // 2, i), landing(grp, sp, i), send.at[i, k], recv.at[i, k], "sp", to
+        )
+
+    def arrived(grp, k, i):
+        source = flip(sp, k)
+        block = landing(grp, source, i)
+        remote(block, block, send.at[i, k], recv.at[i, k], "sp", source).wait_recv()
+
+    my_group, my_head = group_of(sp), sp // 2
+
+    def send_all(parts):
+        for k in range(1, n_sp):
+            for grp in range(2):
+
+                @pl.when(group_of(flip(sp, k)) == grp)
+                def _():
+                    for i in parts:
+                        qkv(grp, k, i).start()
+
+    for copy in copies[:4]:
+        copy.wait()
+    send_all((1, 2))
+    for copy in copies[4:6]:
+        copy.wait()
+    send_all((0,))
+    for grp in range(2):
+
+        @pl.when(my_group == grp)
+        def _():
+            for i in range(3):
+                landing(grp, sp, i)[...] = piece(grp, my_head, i)[...]
+
+    for copy in copies[6:13]:
+        copy.wait()
+    route(ids, gates, spread, shares, n_sp * experts)
+
+    for grp in range(2):
+
+        @pl.when(my_group == grp)
+        def _():
+            for k in range(1, n_sp):
+                arrived(grp, k, 1)
+                arrived(grp, k, 2)
+
+    factor = jnp.where(my_group == 0, QK_NARROW**-0.5, QK_BROAD**-0.5) * LOG2E
+    lam_row = lam[pl.ds(my_group, 1), :]
+    mixing = jnp.sum(
+        jnp.where(lax.broadcasted_iota(jnp.int32, lam_row.shape, 1) == my_head, lam_row, 0.0),
+        -1,
+        keepdims=True,
+    )
+    gain = gains[pl.ds(my_group, 1), :]
+    span = 2 * count
+    col = my_group * heads + my_head
+    keep_all = jnp.broadcast_to(my_group, (span, lane)) == 1
+    place = lax.broadcasted_iota(jnp.int32, (span, lane), 1) // QK_NARROW
+
+    def head_send_of(k):
+        s = flip(sp, k)
+        return remote(
+            head_out.at[block_rows(s), :], head_in.at[:, lanes(col, lane)],
+            head_send.at[k], head_recv.at[k], "sp", s,
+        )
+
+    for j in range(n_sp // 2):
+        first = flip(sp // 2, j)
+        q_rows = pl.ds(pl.multiple_of(first * span, span), span)
+        for grp in range(2):
+
+            @pl.when(my_group == grp)
+            def _():
+                for k in (2 * j, 2 * j + 1):
+                    if k:
+                        arrived(grp, k, 0)
+
+        parts = []
+        for m in range(2):
+            cut = lanes(my_group * m, lane)
+            queries = q_all[q_rows, cut].astype(f32)
+            queries = jnp.where(keep_all | (place == m), queries, 0.0).astype(bf16)
+            scores = lax.dot_general(
+                queries, k_all[:, cut], (((1,), (1,)), ((), ())), preferred_element_type=f32
+            )
+            highest = jnp.max(scores, -1, keepdims=True)
+            expo = jnp.exp2((scores - highest) * factor)
+            total = jnp.sum(expo, -1, keepdims=True)
+            numer = jnp.dot(expo.astype(bf16), v_all[...], preferred_element_type=f32)
+            parts.append(numer / total)
+        diff = parts[0] - mixing * parts[1]
+        normed = diff * lax.rsqrt(jnp.mean(diff * diff, -1, keepdims=True) + norm_eps) * gain
+        head_out[q_rows, :] = normed.astype(bf16)
+        for k in (2 * j, 2 * j + 1):
+            if k:
+                head_send_of(k).start()
+            else:
+                head_in[:, lanes(col, lane)] = head_out[rows, :]
+
+    for copy in copies[13:]:
+        copy.wait()
+
+    def head_arrived(k):
+        s = flip(sp, k)
+        target = head_in.at[:, lanes(group_of(s) * heads + s // 2, lane)]
+        remote(target, target, head_send.at[k], head_recv.at[k], "sp", s).wait_recv()
+
+    side = heads * lane // 2
+    half = sp // (n_sp // 2)
+
+    def projected(which, cut):
+        at = pl.ds(pl.multiple_of(which * side, side), side)
+        wide = pl.ds(pl.multiple_of(which * side + 2 * side, side), side)
+        return jnp.dot(head_in[:, at], proj_n[at, cut], preferred_element_type=f32) + jnp.dot(
+            head_in[:, wide], proj_b[at, cut], preferred_element_type=f32
+        )
+
+    for k in range(1, n_sp // 2):
+        head_arrived(k)
+    for t in range(n_tp):
+        cut = slice(t * width, (t + 1) * width)
+        early[:, cut] = projected(half, cut)
+    for k in range(n_sp // 2, n_sp):
+        head_arrived(k)
+
+    def quarter(t):
+        cut = lanes(t, width)
+        return early[:, cut] + projected(1 - half, cut)
+
+    def to_partner(i):
+        return remote(pc_out.at[i], pc_in.at[i], pc_send.at[i], pc_recv.at[i], "tp", core)
+
+    def partner(i):
+        remote(pc_in.at[i], pc_in.at[i], pc_send.at[i], pc_recv.at[i], "tp", core).wait_recv()
+        return pc_in[i].astype(f32)
+
+    over = remote(py_out, py_in, py_send.at[0], py_recv.at[0], "tp", far)
+    pc_out[0] = quarter(far_core).astype(bf16)
+    to_partner(0).start()
+    product = quarter(far)
+    pc_out[1] = quarter(core).astype(bf16)
+    to_partner(1).start()
+    py_out[...] = (product + partner(0)).astype(bf16)
+    over.start()
+    summed_own = quarter(tp) + partner(1) + deep_alpha * tok[...].astype(f32)
+    over.wait_recv()
+    full = summed_own + py_in[...].astype(f32)
+
+    center = jnp.mean(full, -1, keepdims=True)
+    apart = full - center
+    squares = jnp.sum(apart * apart, -1, keepdims=True)
+    which = lax.broadcasted_iota(jnp.int32, (count, lane), 1)
+    st_out[...] = jnp.where(which == 0, center, squares).T[: st_out.shape[0]]
+
+    def share_stats(k):
+        to = lax.rem(tp + k, n_tp)
+        return remote(st_out, st_in.at[k], st_send.at[k], st_recv.at[k], "tp", to)
+
+    for k in range(1, n_tp):
+        share_stats(k).start()
+    st_in[0] = st_out[...]
+    for k in range(1, n_tp):
+        share_stats(k).wait_recv()
+    means = [st_in[k, 0:1, :] for k in range(n_tp)]
+    mean = sum(means[1:], means[0]) / n_tp
+    spreads = [
+        st_in[k, 1:2, :] + width * jnp.square(means[k] - mean) for k in range(n_tp)
+    ]
+    scale = lax.rsqrt(sum(spreads[1:], spreads[0]) / (n_tp * width) + norm_eps)
+    upright = jnp.where(
+        lax.broadcasted_iota(jnp.int32, (lane, count), 0) == 0, mean, scale
+    ).T
+    mixed[...] = ((full - upright[:, 0:1]) * upright[:, 1:2] * gain_one[...]).astype(bf16)
+
+    picked = jnp.dot(spread[...], mixed[...], preferred_element_type=f32)
+    rows_out[...] = picked.astype(bf16).reshape(rows_out.shape)
+
+    def dispatch(e, k):
+        to = flip(sp, k)
+        return remote(
+            rows_out.at[to, e], rows_in.at[tp, e, sp], a_send.at[e, k], a_recv.at[e, k], "sp", to
+        )
+
+    def send_rows(e):
+        for k in range(1, n_sp):
+            dispatch(e, k).start()
+        rows_in[tp, e, sp] = rows_out[sp, e]
+
+    each(send_rows)
+
+    def over_y(e):
+        block = rows_in.at[tp, e]
+        return remote(block, block, y_send.at[e], y_recv.at[e], "tp", far)
+
+    def across(e, k):
+        block = rows_in.at[(tp, far)[k], e]
+        return remote(block, block, c_send.at[e, k], c_recv.at[e, k], "tp", core)
+
+    def pass_on(e):
+        for k in range(1, n_sp):
+            source = flip(sp, k)
+            block = rows_in.at[tp, e, source]
+            remote(block, block, a_send.at[e, k], a_recv.at[e, k], "sp", source).wait_recv()
+        over_y(e).start()
+        across(e, 0).start()
+
+    def pass_across(e):
+        block = rows_in.at[far, e]
+        remote(block, block, y_send.at[e], y_recv.at[e], "tp", far).wait_recv()
+        across(e, 1).start()
+
+    def ready(e):
+        for k, t in enumerate((core, far_core)):
+            block = rows_in.at[t, e]
+            remote(block, block, c_send.at[e, k], c_recv.at[e, k], "tp", core).wait_recv()
+
+    def to_core(e, k):
+        t = (core, far_core)[k]
+        return remote(
+            part.at[t, e], part_core.at[k, e], d_send.at[e, k], d_recv.at[e, k], "tp", core
+        )
+
+    def to_far(e):
+        return remote(part.at[far, e], part_far.at[e], s_send.at[e], s_recv.at[e], "tp", far)
+
+    def give_back(e, k):
+        to = flip(sp, k)
+        return remote(
+            summed.at[e, to], back.at[sp, e], b_send.at[e, k], b_recv.at[e, k], "sp", to
+        )
+
+    def core_sum(e, k):
+        block = part_core.at[k, e]
+        remote(block, block, d_send.at[e, k], d_recv.at[e, k], "tp", core).wait_recv()
+        return part[(tp, far)[k], e].astype(f32) + part_core[k, e].astype(f32)
+
+    def reduce_core(e):
+        part[far, e] = core_sum(e, 1).astype(bf16)
+        to_far(e).start()
+
+    def reduce_far(e):
+        total = core_sum(e, 0)
+        block = part_far.at[e]
+        remote(block, block, s_send.at[e], s_recv.at[e], "tp", far).wait_recv()
+        total = total + part_far[e].astype(f32)
+        summed[e] = total.astype(bf16).reshape(n_sp, CAP, width)
+        for k in range(1, n_sp):
+            give_back(e, k).start()
+        back[sp, e] = summed[e, sp]
+
+    tile = min(256, hidden)
+    tiles = hidden // tile
+
+    def compute(e, _):
+        slot = lax.rem(e, slots)
+        load(e, False)
+        ready(e)
+        inputs = jnp.concatenate(
+            [rows_in[t, e].reshape(filled, width) for t in range(n_tp)], axis=1
+        )
+
+        def hidden_tile(j, _):
+            cut = lanes(j, tile)
+            gated = jnp.dot(inputs, gate[slot, :, cut], preferred_element_type=f32)
+            lifted = jnp.dot(inputs, up[slot, :, cut], preferred_element_type=f32)
+            act[:, cut] = (gated / (1.0 + jnp.exp(-gated)) * lifted).astype(bf16)
+            pl.when((j == 0) & (e + 2 < experts))(lambda: pass_on(e + 2))
+            pl.when((j == min(1, tiles - 1)) & (e >= 2))(lambda: reduce_far(e - 2))
+            pl.when((j == min(2, tiles - 1)) & (e + 1 < experts))(lambda: pass_across(e + 1))
+            return 0
+
+        lax.fori_loop(0, tiles, hidden_tile, 0)
+
+        def down_tile(i, _):
+            t = 2 * lax.rem(y + 1 + i // 2, 2) + lax.rem(c + 1 + i, 2)
+            product = jnp.dot(
+                act[...], down[slot, :, lanes(t, width)], preferred_element_type=f32
+            )
+            part[t, e] = product.astype(bf16)
+            pl.when(i == 0)(lambda: to_core(e, 1).start())
+            pl.when(i == 2)(lambda: to_core(e, 0).start())
+            return 0
+
+        lax.fori_loop(0, n_tp, down_tile, 0)
+        pl.when(e + slots < experts)(lambda: load(e + slots, True))
+        reduce_core(e)
+        return 0
+
+    pass_on(0)
+    if experts > 1:
+        pass_on(1)
+    pass_across(0)
+    lax.fori_loop(0, experts, compute, 0)
+    for e in range(max(0, experts - 2), experts):
+        reduce_far(e)
+
+    def arrive(e):
+        for k in range(1, n_sp):
+            source = flip(sp, k)
+            block = back.at[source, e]
+            remote(block, block, b_send.at[e, k], b_recv.at[e, k], "sp", source).wait_recv()
+
+    each(arrive)
+    returned = back[...].reshape(n_sp * experts * CAP, width)
+    routed = jnp.dot(shares[...], returned, preferred_element_type=f32)
+    z_all[tp] = (deep_alpha * mixed[...].astype(f32) + routed).astype(bf16)
+
+    def final(i):
+        t, to = ((tp, far), (tp, core), (far, core))[i]
+        return remote(z_all.at[t], z_all.at[t], g_send.at[i], g_recv.at[i], "tp", to)
+
+    def final_wait(i):
+        t, source = ((far, far), (core, core), (far_core, core))[i]
+        remote(z_all.at[t], z_all.at[t], g_send.at[i], g_recv.at[i], "tp", source).wait_recv()
+
+    final(0).start()
+    final(1).start()
+    final_wait(0)
+    final(2).start()
+    final_wait(1)
+    final_wait(2)
+    members = [z_all[t].astype(f32) for t in range(n_tp)]
+    sums = [jnp.sum(z, -1, keepdims=True) for z in members]
+    middle = sum(sums[1:], sums[0]) / (n_tp * width)
+    members = [z - middle for z in members]
+    sums = [jnp.sum(z * z, -1, keepdims=True) for z in members]
+    stretch = lax.rsqrt(sum(sums[1:], sums[0]) / (n_tp * width) + norm_eps)
+    for t in range(n_tp):
+        cut = slice(t * width, (t + 1) * width)
+        out[:, cut] = (members[t] * stretch * gain_two[:, cut]).astype(bf16)
+
+    for k in range(1, n_sp):
+        for grp in range(2):
+
+            @pl.when(group_of(flip(sp, k)) == grp)
+            def _():
+                for i in range(3):
+                    qkv(grp, k, i).wait_send()
+
+        head_send_of(k).wait_send()
+    for i in range(2):
+        to_partner(i).wait_send()
+    over.wait_send()
+    for k in range(1, n_tp):
+        share_stats(k).wait_send()
+
+    def sent(e):
+        for k in range(1, n_sp):
+            dispatch(e, k).wait_send()
+            give_back(e, k).wait_send()
+        over_y(e).wait_send()
+        for k in range(2):
+            across(e, k).wait_send()
+            to_core(e, k).wait_send()
+        to_far(e).wait_send()
+
+    each(sent)
+    for i in range(3):
+        final(i).wait_send()
+
+
+def layer_rows(
+    tokens, qn, kn, vn, qb, kb, vb, mix_lambda, head_gain, proj_n, proj_b, gain_one, gain_two,
+    expert_ids, expert_gates, wg, wu, wd,
+):
+    n_sp, n_tp = lax.axis_size("sp"), lax.axis_size("tp")
+    count, model_width = tokens.shape
+    heads = vn.shape[1] // V
+    width = model_width // n_tp
+    experts, hidden = wg.shape[0], wg.shape[2]
+    slots = min(3, experts)
+    filled = n_sp * CAP
+    places = n_sp * experts * CAP
+    bf16, f32 = jnp.bfloat16, jnp.float32
+    dma = pltpu.SemaphoreType.DMA
+    far = pl.BlockSpec(memory_space=pltpu.HBM)
+    near = pl.BlockSpec(memory_space=pltpu.VMEM)
+    vmem = lambda *shape: pltpu.VMEM(shape, bf16)
+    wide = lambda *shape: pltpu.VMEM(shape, f32)
+    like = lambda array: pltpu.VMEM(array.shape, array.dtype)
+    ids, gates = expert_ids.T, expert_gates.T
+    one, two = gain_one[None, :], gain_two[None, :]
+    operands = (
+        mix_lambda, ids, gates, tokens, qn, kn, vn, qb, kb, vb, head_gain, proj_n, proj_b,
+        one, two, wg, wu, wd,
+    )
+    return pl.pallas_call(
+        functools.partial(layer_kernel, n_sp, n_tp, heads),
+        out_shape=jax.ShapeDtypeStruct(tokens.shape, bf16),
+        in_specs=[far] * len(operands),
+        out_specs=near,
+        scratch_shapes=[
+            like(mix_lambda),
+            like(ids),
+            like(gates),
+            vmem(count, width),
+            like(qn),
+            like(kn),
+            like(vn),
+            like(qb),
+            like(kb),
+            like(vb),
+            like(head_gain),
+            like(proj_n),
+            like(proj_b),
+            wide(1, width),
+            like(two),
+            vmem(slots, *wg.shape[1:]),
+            vmem(slots, *wu.shape[1:]),
+            vmem(slots, *wd.shape[1:]),
+            vmem(n_sp * count, 2 * V),
+            vmem(n_sp * count, 2 * V),
+            vmem(n_sp * count, V),
+            vmem(n_sp * count, V),
+            vmem(count, 2 * heads * V),
+            wide(count, model_width),
+            vmem(2, count, width),
+            vmem(2, count, width),
+            vmem(count, width),
+            vmem(count, width),
+            wide(8, count),
+            wide(n_tp, 8, count),
+            vmem(count, width),
+            vmem(places, count),
+            vmem(count, places),
+            vmem(n_sp, experts, CAP, width),
+            vmem(n_tp, experts, n_sp, CAP, width),
+            vmem(filled, hidden),
+            vmem(n_tp, experts, filled, width),
+            vmem(2, experts, filled, width),
+            vmem(experts, filled, width),
+            vmem(experts, n_sp, CAP, width),
+            vmem(n_sp, experts, CAP, width),
+            vmem(n_tp, count, width),
+            dma((15,)),
+            dma((3, slots)),
+            dma((3, n_sp)),
+            dma((3, n_sp)),
+            dma((n_sp,)),
+            dma((n_sp,)),
+        ]
+        + [dma((2,))] * 2
+        + [dma((1,))] * 2
+        + [dma((n_tp,))] * 2
+        + [dma((experts, n_sp))] * 2
+        + [dma((experts,))] * 2
+        + [dma((experts, 2))] * 4
+        + [dma((experts,))] * 2
+        + [dma((experts, n_sp))] * 2
+        + [dma((3,))] * 2,
+        compiler_params=pltpu.CompilerParams(
+            collective_id=0, has_side_effects=True, vmem_limit_bytes=61 * 2**20
+        ),
+        name="layer",
+    )(*operands)
+
+
 def head_fold(running, queries, key_rows, values, key_width):
     maxima, totals, weighted = running
     length = key_rows.shape[0]
@@ -629,8 +967,13 @@
         proj_broad,
         gain_one,
     )
-    whole_heads = 2 * (value_narrow.shape[1] // V) == lax.axis_size("sp")
-    mixed_rows = (attention_rows if whole_heads else attention_gathered)(*members)
+    n_sp, n_tp = lax.axis_size("sp"), lax.axis_size("tp")
+    whole_heads = 2 * (value_narrow.shape[1] // V) == n_sp
+    if whole_heads and n_tp // 2 == 2 and not n_sp & (n_sp - 1):
+        return layer_rows(
+            *members, gain_two, expert_ids, expert_gates, gate_weight, up_weight, down_weight
+        )
+    mixed_rows = attention_gathered(*members)
     experts_all = gate_weight.shape[0] * lax.axis_size("sp")
     chosen = expert_ids.reshape(-1)
     onehot = (chosen[:, None] == jnp.arange(experts_all, dtype=jnp.int32)[None, :]).astype(

time: 132 us -> 97.5 us (0.74)
  Pallas kernels: 111 us -> 95.4 us
  local copies, waits for them, and re-layouts: 16.1 us -> 1.88 us
  other arithmetic: 3.81 us -> 0 us
    pallas_call x2 -> x1, Pallas kernels: 111 us -> 95.4 us  [layer_rows(): pl.pallas_call(functools.partial(layer_kernel, n_sp, n_tp, heads), out_sh...]
    unnamed x28 -> x1, local copies, waits for them, and re-layouts: 15.2 us -> 1.88 us
    convert_element_type x3 -> x0, other arithmetic: 1.42 us -> none  [the longest x1 0.74 us: on_device(): low = (shares - high).astype(jnp.bfloat16)]
where the time goes in v1:
time: 97.5 us; the launch traced here: 97.3 us
  Pallas kernels  95.4 us (98%)
  local copies, waits for them, and re-layouts  1.88 us (2%)
    pallas_call x1, Pallas kernels, layer_rows(): pl.pallas_call(functools.partial(layer_kernel, n_sp, n_tp, heads), out_sh...  95.4 us

profile of v1, /device:TPU:1, one launch (start us, length us, event | category | flops | bytes accessed | tf_op | source)
XLA Modules:
  0.0 97.3 jit_solution(1879816379152092298)
XLA Ops:
  0.0 95.4 %layer.1 = bf16[128,2048]{1,0:T(8,128)(2,1)} custom-call(f32[2,4]{1,0:T(2,128)} %lam_h.1, s32[2,128]{1,0:T(2,128)} %bitcast.6, f32[2,128]{1,0:T(2,128)} %bitcast.7, bf16[128,2048]{1,0:T(8,128)(2,1)} %tok_h.1, bf16[128,512]{1,0:T(8,128)(2,1)} %qn_h.1, bf16[128,512]{1,0:T(8,128)(2,1)} %kn_h.1, bf16[128,512]{1,0:T(8,128)(2,1)} %vn_h.1, bf16[128,1024]{1,0:T(8,128)(2,1)} %qb_h.1, ...), custom_call_target="tpu_custom_call" | custom-call | tf_op jit(solution)/shard_map/layer/pallas_call | solution.py:782
  95.4 1.9 %copy.20 = bf16[128,2048]{1,0:T(8,128)(2,1)} copy(bf16[128,2048]{1,0:T(8,128)(2,1)} %layer.1) | data formatting | bytes 1048576

commit v2 on v1

--- a/solution.py
+++ b/solution.py
@@ -302,7 +302,7 @@
     return index
 
 
-def route(ids, gates, spread, shares, experts_all):
+def route(ids, gates, spread, shares, experts_all, owners):
     count = ids.shape[1]
     expert = lax.broadcasted_iota(jnp.int32, (experts_all, count), 0)
     picks = [(expert == ids[k : k + 1, :]).astype(jnp.float32) for k in range(TOP)]
@@ -320,7 +320,9 @@
     marked = jnp.zeros((experts_all * CAP, count), jnp.float32)
     for k in range(TOP):
         slot = jnp.sum(before * picks[k], 0, keepdims=True)
-        position = ids[k : k + 1, :].astype(jnp.float32) * CAP + slot
+        chosen, own = ids[k : k + 1, :], experts_all // owners
+        order = lax.rem(chosen, own) * owners + chosen // own
+        position = order.astype(jnp.float32) * CAP + slot
         hit = place == position
         weight = weight + jnp.where(hit, gates[k : k + 1, :], 0.0)
         marked = marked + jnp.where(hit, 1.0, 0.0)
@@ -405,8 +407,14 @@
 
     my_group, my_head = group_of(sp), sp // 2
 
+    near = n_sp // 2
+    order = [*range(near - 1, 0, -1), *range(n_sp - 1, near - 1, -1)]
+
+    def side_order(g):
+        return order[near - 1 :] if g else order[: near - 1]
+
     def send_all(parts):
-        for k in range(1, n_sp):
+        for k in order:
             for grp in range(2):
 
                 @pl.when(group_of(flip(sp, k)) == grp)
@@ -429,7 +437,7 @@
 
     for copy in copies[6:13]:
         copy.wait()
-    route(ids, gates, spread, shares, n_sp * experts)
+    route(ids, gates, spread, shares, n_sp * experts, n_sp)
 
     for grp in range(2):
 
@@ -447,10 +455,7 @@
         keepdims=True,
     )
     gain = gains[pl.ds(my_group, 1), :]
-    span = 2 * count
     col = my_group * heads + my_head
-    keep_all = jnp.broadcast_to(my_group, (span, lane)) == 1
-    place = lax.broadcasted_iota(jnp.int32, (span, lane), 1) // QK_NARROW
 
     def head_send_of(k):
         s = flip(sp, k)
@@ -459,17 +464,20 @@
             head_send.at[k], head_recv.at[k], "sp", s,
         )
 
-    for j in range(n_sp // 2):
-        first = flip(sp // 2, j)
-        q_rows = pl.ds(pl.multiple_of(first * span, span), span)
+    def attend(ks):
         for grp in range(2):
 
             @pl.when(my_group == grp)
             def _():
-                for k in (2 * j, 2 * j + 1):
+                for k in ks:
                     if k:
                         arrived(grp, k, 0)
 
+        span = len(ks) * count
+        first = flip(sp, ks[0]) // len(ks)
+        q_rows = pl.ds(pl.multiple_of(first * span, span), span)
+        keep_all = jnp.broadcast_to(my_group, (span, lane)) == 1
+        place = lax.broadcasted_iota(jnp.int32, (span, lane), 1) // QK_NARROW
         parts = []
         for m in range(2):
             cut = lanes(my_group * m, lane)
@@ -486,11 +494,14 @@
         diff = parts[0] - mixing * parts[1]
         normed = diff * lax.rsqrt(jnp.mean(diff * diff, -1, keepdims=True) + norm_eps) * gain
         head_out[q_rows, :] = normed.astype(bf16)
-        for k in (2 * j, 2 * j + 1):
+        for k in ks[::-1]:
             if k:
                 head_send_of(k).start()
             else:
                 head_in[:, lanes(col, lane)] = head_out[rows, :]
+
+    for k in (*range(0, near, 2), *range(n_sp - 2, near - 1, -2)):
+        attend((k, k + 1))
 
     for copy in copies[13:]:
         copy.wait()
@@ -567,47 +578,54 @@
     ).T
     mixed[...] = ((full - upright[:, 0:1]) * upright[:, 1:2] * gain_one[...]).astype(bf16)
 
-    picked = jnp.dot(spread[...], mixed[...], preferred_element_type=f32)
-    rows_out[...] = picked.astype(bf16).reshape(rows_out.shape)
 
     def dispatch(e, k):
         to = flip(sp, k)
         return remote(
-            rows_out.at[to, e], rows_in.at[tp, e, sp], a_send.at[e, k], a_recv.at[e, k], "sp", to
+            rows_out.at[e, to], rows_in.at[tp, e, sp], a_send.at[e, k], a_recv.at[e, k], "sp", to
         )
 
     def send_rows(e):
-        for k in range(1, n_sp):
+        at = pl.ds(pl.multiple_of(e * filled, filled), filled)
+        picked = jnp.dot(spread[at, :], mixed[...], preferred_element_type=f32)
+        rows_out[e] = picked.astype(bf16).reshape(rows_out.shape[1:])
+        for k in order:
             dispatch(e, k).start()
-        rows_in[tp, e, sp] = rows_out[sp, e]
+        rows_in[tp, e, sp] = rows_out[e, sp]
 
     each(send_rows)
 
-    def over_y(e):
-        block = rows_in.at[tp, e]
-        return remote(block, block, y_send.at[e], y_recv.at[e], "tp", far)
-
-    def across(e, k):
-        block = rows_in.at[(tp, far)[k], e]
-        return remote(block, block, c_send.at[e, k], c_recv.at[e, k], "tp", core)
-
-    def pass_on(e):
-        for k in range(1, n_sp):
+    def side_of(g):
+        return pl.ds(pl.multiple_of((half if g == 0 else 1 - half) * near, near), near)
+
+    def over_y(e, g):
+        block = rows_in.at[tp, e, side_of(g)]
+        return remote(block, block, y_send.at[e, g], y_recv.at[e, g], "tp", far)
+
+    def across(e, k, g):
+        block = rows_in.at[(tp, far)[k], e, side_of(g)]
+        i = 2 * k + g
+        return remote(block, block, c_send.at[e, i], c_recv.at[e, i], "tp", core)
+
+    def pass_on(e, g):
+        for k in side_order(g):
             source = flip(sp, k)
             block = rows_in.at[tp, e, source]
             remote(block, block, a_send.at[e, k], a_recv.at[e, k], "sp", source).wait_recv()
-        over_y(e).start()
-        across(e, 0).start()
-
-    def pass_across(e):
-        block = rows_in.at[far, e]
-        remote(block, block, y_send.at[e], y_recv.at[e], "tp", far).wait_recv()
-        across(e, 1).start()
+        over_y(e, g).start()
+        across(e, 0, g).start()
+
+    def pass_across(e, g):
+        block = rows_in.at[far, e, side_of(g)]
+        remote(block, block, y_send.at[e, g], y_recv.at[e, g], "tp", far).wait_recv()
+        across(e, 1, g).start()
 
     def ready(e):
         for k, t in enumerate((core, far_core)):
-            block = rows_in.at[t, e]
-            remote(block, block, c_send.at[e, k], c_recv.at[e, k], "tp", core).wait_recv()
+            for g in range(2):
+                block = rows_in.at[t, e, side_of(g)]
+                i = 2 * k + g
+                remote(block, block, c_send.at[e, i], c_recv.at[e, i], "tp", core).wait_recv()
 
     def to_core(e, k):
         t = (core, far_core)[k]
@@ -615,35 +633,49 @@
             part.at[t, e], part_core.at[k, e], d_send.at[e, k], d_recv.at[e, k], "tp", core
         )
 
-    def to_far(e):
-        return remote(part.at[far, e], part_far.at[e], s_send.at[e], s_recv.at[e], "tp", far)
+    def rows_for(g):
+        size = near * CAP
+        return pl.ds(pl.multiple_of((half if g == 0 else 1 - half) * size, size), size)
+
+    def to_far(e, g):
+        at = rows_for(g)
+        return remote(
+            part.at[far, e, at], part_far.at[e, at], s_send.at[e, g], s_recv.at[e, g], "tp", far
+        )
 
     def give_back(e, k):
         to = flip(sp, k)
         return remote(
-            summed.at[e, to], back.at[sp, e], b_send.at[e, k], b_recv.at[e, k], "sp", to
-        )
-
-    def core_sum(e, k):
+            summed.at[e, to], back.at[e, sp], b_send.at[e, k], b_recv.at[e, k], "sp", to
+        )
+
+    def core_arrived(e, k):
         block = part_core.at[k, e]
         remote(block, block, d_send.at[e, k], d_recv.at[e, k], "tp", core).wait_recv()
-        return part[(tp, far)[k], e].astype(f32) + part_core[k, e].astype(f32)
-
-    def reduce_core(e):
-        part[far, e] = core_sum(e, 1).astype(bf16)
-        to_far(e).start()
-
-    def reduce_far(e):
-        total = core_sum(e, 0)
-        block = part_far.at[e]
-        remote(block, block, s_send.at[e], s_recv.at[e], "tp", far).wait_recv()
-        total = total + part_far[e].astype(f32)
-        summed[e] = total.astype(bf16).reshape(n_sp, CAP, width)
-        for k in range(1, n_sp):
+
+    def reduce_core(e, g):
+        if g == 1:
+            core_arrived(e, 1)
+        at = rows_for(g)
+        total = part[far, e, at].astype(f32) + part_core[1, e, at].astype(f32)
+        part[far, e, at] = total.astype(bf16)
+        to_far(e, g).start()
+
+    def reduce_far(e, g):
+        if g == 1:
+            core_arrived(e, 0)
+        at = rows_for(g)
+        block = part_far.at[e, at]
+        remote(block, block, s_send.at[e, g], s_recv.at[e, g], "tp", far).wait_recv()
+        total = part[tp, e, at].astype(f32) + part_core[0, e, at].astype(f32)
+        total = total + part_far[e, at].astype(f32)
+        summed[e, side_of(g)] = total.astype(bf16).reshape(near, CAP, width)
+        for k in side_order(g):
             give_back(e, k).start()
-        back[sp, e] = summed[e, sp]
-
-    tile = min(256, hidden)
+        if g == 0:
+            back[e, sp] = summed[e, sp]
+
+    tile = min(512, hidden)
     tiles = hidden // tile
 
     def compute(e, _):
@@ -659,12 +691,19 @@
             gated = jnp.dot(inputs, gate[slot, :, cut], preferred_element_type=f32)
             lifted = jnp.dot(inputs, up[slot, :, cut], preferred_element_type=f32)
             act[:, cut] = (gated / (1.0 + jnp.exp(-gated)) * lifted).astype(bf16)
-            pl.when((j == 0) & (e + 2 < experts))(lambda: pass_on(e + 2))
-            pl.when((j == min(1, tiles - 1)) & (e >= 2))(lambda: reduce_far(e - 2))
-            pl.when((j == min(2, tiles - 1)) & (e + 1 < experts))(lambda: pass_across(e + 1))
+            pl.when(j == 0)(lambda: between(e))
             return 0
 
+        def between(e):
+            pl.when(e + 2 < experts)(lambda: pass_on(e + 2, 1))
+            pl.when(e + 3 < experts)(lambda: pass_on(e + 3, 0))
+            pl.when(e >= 1)(lambda: reduce_core(e - 1, 0))
+            pl.when(e >= 2)(lambda: reduce_far(e - 2, 1))
+
         lax.fori_loop(0, tiles, hidden_tile, 0)
+        for g in range(2):
+            pl.when(e + 1 < experts)(lambda: pass_across(e + 1, g))
+        pl.when(e >= 2)(lambda: reduce_far(e - 2, 0))
 
         def down_tile(i, _):
             t = 2 * lax.rem(y + 1 + i // 2, 2) + lax.rem(c + 1 + i, 2)
@@ -678,27 +717,39 @@
 
         lax.fori_loop(0, n_tp, down_tile, 0)
         pl.when(e + slots < experts)(lambda: load(e + slots, True))
-        reduce_core(e)
+        reduce_core(e, 1)
         return 0
 
-    pass_on(0)
+    pass_on(0, 0)
     if experts > 1:
-        pass_on(1)
-    pass_across(0)
+        pass_on(1, 0)
+    pass_on(0, 1)
+    pass_across(0, 0)
+    if experts > 1:
+        pass_on(1, 1)
+    if experts > 2:
+        pass_on(2, 0)
+    pass_across(0, 1)
     lax.fori_loop(0, experts, compute, 0)
-    for e in range(max(0, experts - 2), experts):
-        reduce_far(e)
-
-    def arrive(e):
-        for k in range(1, n_sp):
+    reduce_core(experts - 1, 0)
+    for g in (1, 0):
+        for e in range(max(0, experts - 2), experts):
+            reduce_far(e, g)
+
+    def arrive(e, total):
+        for k in order:
             source = flip(sp, k)
-            block = back.at[source, e]
+            block = back.at[e, source]
             remote(block, block, b_send.at[e, k], b_recv.at[e, k], "sp", source).wait_recv()
-
-    each(arrive)
-    returned = back[...].reshape(n_sp * experts * CAP, width)
-    routed = jnp.dot(shares[...], returned, preferred_element_type=f32)
-    z_all[tp] = (deep_alpha * mixed[...].astype(f32) + routed).astype(bf16)
+        at = slice(e * filled, (e + 1) * filled)
+        return total + jnp.dot(
+            shares[:, at], back[e].reshape(filled, width), preferred_element_type=f32
+        )
+
+    total = deep_alpha * mixed[...].astype(f32)
+    for e in range(experts):
+        total = arrive(e, total)
+    z_all[tp] = total.astype(bf16)
 
     def final(i):
         t, to = ((tp, far), (tp, core), (far, core))[i]
@@ -743,11 +794,12 @@
         for k in range(1, n_sp):
             dispatch(e, k).wait_send()
             give_back(e, k).wait_send()
-        over_y(e).wait_send()
         for k in range(2):
-            across(e, k).wait_send()
+            over_y(e, k).wait_send()
+            across(e, 0, k).wait_send()
+            across(e, 1, k).wait_send()
             to_core(e, k).wait_send()
-        to_far(e).wait_send()
+            to_far(e, k).wait_send()
 
     each(sent)
     for i in range(3):
@@ -781,7 +833,7 @@
     )
     return pl.pallas_call(
         functools.partial(layer_kernel, n_sp, n_tp, heads),
-        out_shape=jax.ShapeDtypeStruct(tokens.shape, bf16),
+        out_shape=pltpu.VMEM(tokens.shape, bf16),
         in_specs=[far] * len(operands),
         out_specs=near,
         scratch_shapes=[
@@ -818,14 +870,14 @@
             vmem(count, width),
             vmem(places, count),
             vmem(count, places),
-            vmem(n_sp, experts, CAP, width),
+            vmem(experts, n_sp, CAP, width),
             vmem(n_tp, experts, n_sp, CAP, width),
             vmem(filled, hidden),
             vmem(n_tp, experts, filled, width),
             vmem(2, experts, filled, width),
             vmem(experts, filled, width),
             vmem(experts, n_sp, CAP, width),
-            vmem(n_sp, experts, CAP, width),
+            vmem(experts, n_sp, CAP, width),
             vmem(n_tp, count, width),
             dma((15,)),
             dma((3, slots)),
@@ -838,9 +890,9 @@
         + [dma((1,))] * 2
         + [dma((n_tp,))] * 2
         + [dma((experts, n_sp))] * 2
-        + [dma((experts,))] * 2
+        + [dma((experts, 2))] * 2
+        + [dma((experts, 4))] * 2
         + [dma((experts, 2))] * 4
-        + [dma((experts,))] * 2
         + [dma((experts, n_sp))] * 2
         + [dma((3,))] * 2,
         compiler_params=pltpu.CompilerParams(

time: 97.5 us -> 90.8 us (0.931)
  Pallas kernels: 95.4 us -> 89.8 us
  local copies, waits for them, and re-layouts: 1.88 us -> 0.8 us
    pallas_call x1, Pallas kernels: 95.4 us -> 89.8 us  [layer_rows(): pl.pallas_call(functools.partial(layer_kernel, n_sp, n_tp, heads), out_sh...]
    unnamed x1, local copies, waits for them, and re-layouts: 1.88 us -> 0.8 us
where the time goes in v2:
time: 90.8 us; the launch traced here: 90.6 us
  Pallas kernels  89.8 us (99%)
    pallas_call x1, Pallas kernels, layer_rows(): pl.pallas_call(functools.partial(layer_kernel, n_sp, n_tp, heads), out_sh...  89.8 us

profile of v2, /device:TPU:1, one launch (start us, length us, event | category | flops | bytes accessed | tf_op | source)
XLA Modules:
  0.0 90.6 jit_solution(16843532345044215785)
XLA Ops:
  0.0 89.8 %layer.1 = bf16[128,2048]{1,0:T(8,128)(2,1)S(1)} custom-call(f32[2,4]{1,0:T(2,128)} %lam_h.1, s32[2,128]{1,0:T(2,128)} %bitcast.6, f32[2,128]{1,0:T(2,128)} %bitcast.7, bf16[128,2048]{1,0:T(8,128)(2,1)} %tok_h.1, bf16[128,512]{1,0:T(8,128)(2,1)} %qn_h.1, bf16[128,512]{1,0:T(8,128)(2,1)} %kn_h.1, bf16[128,512]{1,0:T(8,128)(2,1)} %vn_h.1, ...), custom_call_target="tpu_custom_call" | custom-call | tf_op jit(solution)/shard_map/layer/pallas_call | solution.py:834
  89.8 0.8 copy.20

commit v3 on v2

--- a/solution.py
+++ b/solution.py
@@ -676,7 +676,6 @@
             back[e, sp] = summed[e, sp]
 
     tile = min(512, hidden)
-    tiles = hidden // tile
 
     def compute(e, _):
         slot = lax.rem(e, slots)
@@ -686,38 +685,33 @@
             [rows_in[t, e].reshape(filled, width) for t in range(n_tp)], axis=1
         )
 
-        def hidden_tile(j, _):
-            cut = lanes(j, tile)
+        for j in range(hidden // tile):
+            cut = slice(j * tile, (j + 1) * tile)
             gated = jnp.dot(inputs, gate[slot, :, cut], preferred_element_type=f32)
             lifted = jnp.dot(inputs, up[slot, :, cut], preferred_element_type=f32)
             act[:, cut] = (gated / (1.0 + jnp.exp(-gated)) * lifted).astype(bf16)
-            pl.when(j == 0)(lambda: between(e))
-            return 0
-
-        def between(e):
-            pl.when(e + 2 < experts)(lambda: pass_on(e + 2, 1))
-            pl.when(e + 3 < experts)(lambda: pass_on(e + 3, 0))
-            pl.when(e >= 1)(lambda: reduce_core(e - 1, 0))
-            pl.when(e >= 2)(lambda: reduce_far(e - 2, 1))
-
-        lax.fori_loop(0, tiles, hidden_tile, 0)
-        for g in range(2):
-            pl.when(e + 1 < experts)(lambda: pass_across(e + 1, g))
-        pl.when(e >= 2)(lambda: reduce_far(e - 2, 0))
-
-        def down_tile(i, _):
-            t = 2 * lax.rem(y + 1 + i // 2, 2) + lax.rem(c + 1 + i, 2)
+        pl.when(e + 2 < experts)(lambda: pass_on(e + 2, 1))
+        pl.when(e + 3 < experts)(lambda: pass_on(e + 3, 0))
+
+        @pl.when(e + 1 < experts)
+        def _():
+            pass_across(e + 1, 0)
+            pl.when(e + 2 < experts)(lambda: pass_across(e + 1, 1))
+
+        pl.when(e >= 2)(lambda: reduce_far(e - 2, 1))
+        pl.when(e >= 1)(lambda: reduce_core(e - 1, 0))
+        pl.when(e >= 3)(lambda: reduce_far(e - 3, 0))
+
+        for i, t in enumerate((far_core, far, core, tp)):
             product = jnp.dot(
                 act[...], down[slot, :, lanes(t, width)], preferred_element_type=f32
             )
             part[t, e] = product.astype(bf16)
-            pl.when(i == 0)(lambda: to_core(e, 1).start())
-            pl.when(i == 2)(lambda: to_core(e, 0).start())
-            return 0
-
-        lax.fori_loop(0, n_tp, down_tile, 0)
+            if i in (0, 2):
+                to_core(e, 1 - i // 2).start()
         pl.when(e + slots < experts)(lambda: load(e + slots, True))
         reduce_core(e, 1)
+        pl.when(e + 2 == experts)(lambda: pass_across(e + 1, 1))
         return 0
 
     pass_on(0, 0)
@@ -731,10 +725,14 @@
         pass_on(2, 0)
     pass_across(0, 1)
     lax.fori_loop(0, experts, compute, 0)
+    last = range(max(0, experts - 2), experts)
     reduce_core(experts - 1, 0)
-    for g in (1, 0):
-        for e in range(max(0, experts - 2), experts):
-            reduce_far(e, g)
+    for e in last:
+        reduce_far(e, 1)
+        if e + 1 < experts and experts > 2:
+            reduce_far(experts - 3, 0)
+    for e in last:
+        reduce_far(e, 0)
 
     def arrive(e, total):
         for k in order:

time: 90.8 us -> 89.7 us (0.988)
  Pallas kernels: 89.8 us -> 88.8 us
    pallas_call x1, Pallas kernels: 89.8 us -> 88.8 us  [layer_rows(): pl.pallas_call(functools.partial(layer_kernel, n_sp, n_tp, heads), out_sh...]
where the time goes in v3:
time: 89.7 us; the launch traced here: 89.6 us
  Pallas kernels  88.8 us (99%)
    pallas_call x1, Pallas kernels, layer_rows(): pl.pallas_call(functools.partial(layer_kernel, n_sp, n_tp, heads), out_sh...  88.8 us

profile of v3, /device:TPU:1, one launch (start us, length us, event | category | flops | bytes accessed | tf_op | source)
XLA Modules:
  0.0 89.6 jit_solution(16199133977585844582)
XLA Ops:
  0.0 88.8 %layer.1 = bf16[128,2048]{1,0:T(8,128)(2,1)S(1)} custom-call(f32[2,4]{1,0:T(2,128)} %lam_h.1, s32[2,128]{1,0:T(2,128)} %bitcast.6, f32[2,128]{1,0:T(2,128)} %bitcast.7, bf16[128,2048]{1,0:T(8,128)(2,1)} %tok_h.1, bf16[128,512]{1,0:T(8,128)(2,1)} %qn_h.1, bf16[128,512]{1,0:T(8,128)(2,1)} %kn_h.1, bf16[128,512]{1,0:T(8,128)(2,1)} %vn_h.1, ...), custom_call_target="tpu_custom_call" | custom-call | tf_op jit(solution)/shard_map/layer/pallas_call | solution.py:832
  88.8 0.8 copy.20
